TPU v7x, 32 devices: a whole 2x2x4 slice. The times are simulated.
32 devices in a mesh: grp: 2 (over y), sp: 4 (over z), tp: 4 (over x, core).
Axes of the slice: x: 2, y: 2, z: 4, core: 2. Of those that a mesh axis runs over, the one named last changes fastest.
Arguments:
- tokens: bfloat16 [1024, 2048], P(('grp', 'sp')), parts along dimension 0, may hold values from -8 to 8
- norm_gain: float32 [2048], replicated, may hold values from 0.1 to 1.9
- w_query: bfloat16 [2048, 1024], P(None, 'tp'), may hold values from -0.125 to 0.125
- w_key: bfloat16 [2048, 1024], P(None, 'tp'), may hold values from -0.125 to 0.125
- w_value: bfloat16 [2048, 1024], P(None, 'tp'), may hold values from -0.125 to 0.125
- w_out: bfloat16 [1024, 2048], P('tp'), may hold values from -0.1875 to 0.1875
- key_rate: bfloat16 [16, 1024], P('tp', ('grp', 'sp')), parts along dimension 1, may hold values from -16 to 1
Outputs:
- layer_out: bfloat16 [1024, 2048], P(('grp', 'sp')), parts along dimension 0
There are 2 independent parts, one for each index of `grp`. A program takes and returns all parts, laid end to end along the dimension named above; an argument that names none is the same for every part. Nothing has to cross between parts.
All inputs are finite; a program needn't handle non-finite values.
Results may differ from a plain program's by a relative error of at most 0.0075.
Values may be sent and summed in bfloat16 or wider, within the bound.
No kernel may reach another device: no remote copies, remote signals or barrier semaphores. Data moves between devices by JAX's collectives and lax.ppermute only.
A program may use at most 64 MiB of HBM per device.

v0:
```python
import jax
import jax.numpy as jnp
from jax import lax
from jax.sharding import PartitionSpec as P

HD = 64
KEY_SPAN = 128
F32 = jnp.float32
BF16 = jnp.bfloat16
HIGHEST = lax.Precision.HIGHEST
EPS = 1e-06


def break_scores(query_heads, key_heads, rate_row_values, query_pos, key_pos):
    scores = jnp.einsum(
        "qhd,khd->hqk", query_heads, key_heads, preferred_element_type=F32
    ) * HD ** (-0.5)
    scores = scores + jnp.transpose(rate_row_values).astype(F32)[:, None, :]
    causal_mask = key_pos[None, :] < query_pos[:, None]
    log_remain = jnp.where(causal_mask[None], jax.nn.log_sigmoid(-scores), 0.0)
    return (scores, causal_mask, log_remain)


def shard_summary(query_heads, key_heads, value_heads, rate_row_values, query_pos, key_pos):
    scores, causal_mask, log_remain = break_scores(
        query_heads, key_heads, rate_row_values, query_pos, key_pos
    )
    heads_here, query_count, key_count = scores.shape
    span_count = key_count // KEY_SPAN
    blocks = log_remain.reshape(heads_here, query_count, span_count, KEY_SPAN)
    span_ids = jnp.arange(KEY_SPAN, dtype=jnp.int32)
    tri_strict = (span_ids[:, None] > span_ids[None, :]).astype(F32)
    inside_sum = jnp.einsum("hqnj,js->hqns", blocks, tri_strict, precision=HIGHEST)
    block_ids = jnp.arange(span_count, dtype=jnp.int32)
    block_later = (block_ids[:, None] > block_ids[None, :]).astype(F32)
    beyond = jnp.einsum("hqn,nm->hqm", jnp.sum(blocks, axis=-1), block_later, precision=HIGHEST)
    suffix = (inside_sum + beyond[..., None]).reshape(heads_here, query_count, key_count)
    weight = jnp.where(causal_mask[None], jnp.exp(jax.nn.log_sigmoid(scores) + suffix), 0.0).astype(
        BF16
    )
    partial_value = jnp.einsum("hqk,khd->qhd", weight, value_heads, preferred_element_type=F32)
    return (partial_value.reshape(query_count, heads_here * HD), jnp.sum(log_remain, axis=-1))


def on_device(tokens, norm_gain, w_query, w_key, w_value, w_out, key_rate):
    tokens_f = tokens.astype(F32)
    normed = (
        tokens_f
        * lax.rsqrt(jnp.mean(tokens_f * tokens_f, axis=-1, keepdims=True) + EPS)
        * norm_gain
    ).astype(BF16)
    queries = jnp.dot(normed, w_query, preferred_element_type=F32).astype(BF16)
    key_rows = jnp.dot(normed, w_key, preferred_element_type=F32).astype(BF16)
    value_rows = jnp.dot(normed, w_value, preferred_element_type=F32).astype(BF16)
    head_width = w_query.shape[1]
    heads_local = head_width // HD
    row_count = tokens.shape[0]
    rate_row_values = jnp.transpose(key_rate)
    query_heads = queries.reshape(row_count, heads_local, HD)
    own_shard = lax.axis_index("sp")
    shard_total = lax.axis_size("sp")
    local_pos = jnp.arange(row_count, dtype=jnp.int32)
    shard_ids = jnp.arange(shard_total, dtype=jnp.int32)
    later_mask = (shard_ids[:, None] > shard_ids[None, :]).astype(F32)
    query_groups = [(query_heads, own_shard * row_count)]

    def summarize(key_block, value_block, rate_block, first_key):
        key_pos = first_key + local_pos
        group_heads, group_start = query_groups[0]
        group_count = group_heads.shape[0]
        group_pos = group_start + jnp.arange(group_count, dtype=jnp.int32)
        empty_pair = (
            jnp.zeros((group_count, head_width), F32),
            jnp.zeros((heads_local, group_count), F32),
        )
        partial_value, remain = lax.cond(
            first_key < group_start + group_count - 1,
            lambda: shard_summary(
                group_heads, key_block, value_block, rate_block, group_pos, key_pos
            ),
            lambda: empty_pair,
        )
        partial_list = [partial_value]
        remain_list = [remain]
        return (jnp.concatenate(partial_list, axis=0), jnp.concatenate(remain_list, axis=1))

    initial = (
        jnp.zeros((shard_total, row_count, head_width), F32),
        jnp.zeros((shard_total, heads_local, row_count), F32),
    )
    piece_keys = lax.all_gather(key_rows, "sp", axis=0, tiled=True)
    piece_values = lax.all_gather(value_rows, "sp", axis=0, tiled=True)
    piece_rates = lax.all_gather(rate_row_values, "sp", axis=0, tiled=True)
    piece_count = piece_keys.shape[0] // row_count
    key_blocks = piece_keys.reshape(piece_count, row_count, heads_local, HD)
    value_blocks = piece_values.reshape(piece_count, row_count, heads_local, HD)
    rate_blocks = piece_rates.reshape(piece_count, row_count, heads_local)

    def absorb_one(inner_pair, item_tuple):
        item_index, key_block, value_block, rate_block = item_tuple
        first_key = item_index * row_count
        shard_index = first_key // row_count
        partial_value, remain = summarize(key_block, value_block, rate_block, first_key)
        partials = lax.dynamic_update_index_in_dim(inner_pair[0], partial_value, shard_index, 0)
        remains = lax.dynamic_update_index_in_dim(inner_pair[1], remain, shard_index, 0)
        return ((partials, remains), None)

    result, _ = lax.scan(
        absorb_one,
        initial,
        (jnp.arange(piece_count, dtype=jnp.int32), key_blocks, value_blocks, rate_blocks),
    )
    partials, remains = result
    beyond = jnp.einsum("nhq,nm->mhq", remains, later_mask, precision=HIGHEST)
    factor = jnp.transpose(jnp.exp(beyond), (0, 2, 1))[..., None]
    mixed_rows = jnp.sum(partials.reshape(shard_total, row_count, heads_local, HD) * factor, axis=0)
    mixed = mixed_rows.reshape(row_count, head_width).astype(BF16)
    token_heads = lax.all_to_all(mixed, "tp", split_axis=0, concat_axis=1, tiled=True)
    whole_out = lax.all_gather(w_out, "tp", axis=0, tiled=True)
    own_rows = jnp.dot(token_heads, whole_out, preferred_element_type=F32).astype(BF16)
    return lax.all_gather(own_rows, "tp", axis=0, tiled=True)


def solution(mesh):
    return jax.shard_map(
        on_device,
        mesh=mesh,
        in_specs=(
            P(("grp", "sp"), None),
            P(),
            P(None, "tp"),
            P(None, "tp"),
            P(None, "tp"),
            P("tp", None),
            P("tp", ("grp", "sp")),
        ),
        out_specs=P(("grp", "sp"), None),
        check_vma=False,
    )
```

profile of v0, /device:TPU:25, one launch (start us, length us, event | category | flops | bytes accessed | tf_op | source)
XLA Modules:
  0.0 93.3 jit_solution(17264272396755167459)
XLA Ops:
  7.3 1.2 %fusion.25 = f32[128]{0:T(128)S(1)} fusion(bf16[128,2048]{1,0:T(8,128)(2,1)} %param.11), kind=kLoop, calls=%fused_computation.40 | loop fusion | flops 786304 | bytes 524800 | tf_op jit(solution)/shard_map/reduce_sum | solution.py:49
  8.5 1.4 %convolution_convert_fusion.3 = bf16[128,256]{1,0:T(8,128)(2,1)S(1)} fusion(bf16[2048,256]{1,0:T(8,128)(2,1)S(1)} %copy-done, bf16[128,2048]{1,0:T(8,128)(2,1)} %param.11, f32[2048]{0:T(1024)} %param.12, f32[128]{0:T(128)S(1)} %add_rsqrt_fusion), kind=kOutput, calls=%fused_computation.37 | convolution fusion | flops 135299072 | bytes 1647104 | tf_op jit(solution)/shard_map/dot_general | solution.py:53
  9.9 11.0 %all_gather.15 = bf16[512,256]{1,0:T(8,128)(2,1)S(1)} all-gather(bf16[128,256]{1,0:T(8,128)(2,1)S(1)} %convolution_convert_fusion.3), channel_id=1, replica_groups=mesh['grp'=2,'sp'=4,'tp'=4] {'sp'}, dimensions={0}, use_global_device_ids=true | all-gather | bytes 327680 | tf_op jit(solution)/shard_map/all_gather | solution.py:91
  21.5 1.6 %convolution_convert_fusion.1 = bf16[128,256]{1,0:T(8,128)(2,1)S(1)} fusion(bf16[2048,256]{1,0:T(8,128)(2,1)} %param.15, bf16[128,2048]{1,0:T(8,128)(2,1)S(1)} %copy-done.1, f32[2048]{0:T(1024)S(1)} %copy-done.3, f32[128]{0:T(128)S(1)} %add_rsqrt_fusion), kind=kOutput, calls=%fused_computation.35 | convolution fusion | flops 135299072 | bytes 1647104 | tf_op jit(solution)/shard_map/dot_general | solution.py:54
  23.1 12.0 %all_gather.17 = bf16[512,256]{1,0:T(8,128)(2,1)S(1)} all-gather(bf16[128,256]{1,0:T(8,128)(2,1)S(1)} %convolution_convert_fusion.1), channel_id=1, replica_groups=mesh['grp'=2,'sp'=4,'tp'=4] {'sp'}, dimensions={0}, use_global_device_ids=true | all-gather | bytes 327680 | tf_op jit(solution)/shard_map/all_gather | solution.py:92
  35.6 1.6 %convolution_convert_fusion.2 = bf16[128,256]{1,0:T(8,128)(2,1)S(1)} fusion(bf16[2048,256]{1,0:T(8,128)(2,1)} %param.13, bf16[128,2048]{1,0:T(8,128)(2,1)S(1)} %copy-done.1, f32[2048]{0:T(1024)S(1)} %copy-done.3, f32[128]{0:T(128)S(1)} %add_rsqrt_fusion), kind=kOutput, calls=%fused_computation.36 | convolution fusion | flops 135299072 | bytes 1647104 | tf_op jit(solution)/shard_map/dot_general | solution.py:52
  37.3 5.6 %all_gather.16 = bf16[512,4]{0,1:T(4,128)(2,1)S(1)} all-gather(bf16[128,4]{0,1:T(4,128)(2,1)S(1)} %bitcast.58), channel_id=1, replica_groups=mesh['grp'=2,'sp'=4,'tp'=4] {'sp'}, dimensions={0}, use_global_device_ids=true | all-gather | bytes 5120 | tf_op jit(solution)/shard_map/all_gather | solution.py:93
  43.0 18.4 %while.16 = (s32[]{:T(128)}, f32[4,128,256]{1,2,0:T(8,128)S(1)}, f32[4,4,128]{2,0,1:T(4,128)S(1)}, s32[4]{0:T(128)S(1)}, s32[]{:T(128)}, /*index=5*/s32[]{:T(128...) while((s32[]{:T(128)}, f32[4,128,256]{1,2,0:T(8,128)S(1)}, ...), condition=%wide.region_5.6_spmd.clone, body=%wide.region_1.5_spmd.clone.sunk | while | flops 119505664 | bytes 1446895 | solution.py:108
  44.3 2.6 %conditional.3 = (f32[1,128,256]{1,2,0:T(8,128)S(1)}, f32[1,4,128]{2,1,0:T(4,128)}) conditional(s32[]{:T(128)} %convert_element_type.82, () %tuple.61, (s32[]{:T(128)}, s32[128]{0:T(128)S(1)}, s32[]{:T(128)}, s32[128]{0:T(128)S(1)}, bf16[4,128,4,64]{1,3,2,0:T(8,128)(2,1)S(1)}, /*index=5*/s32[]{:T(128)}, bf16[128,4,64]{0,2,1:T(8,128)(2,1)S(1)}, ...), branch_computations={%region_2.2_spmd, %region_3.4_spmd} | conditional | flops 119505664 | bytes 1179684 | solution.py:76
  44.4 1.0 %fusion.11 = (f32[4,128]{1,0:T(4,128)}, f32[4,128,128]{1,2,0:T(8,128)S(1)}) fusion(pred[128,128]{0,1:T(8,128)(4,1)S(1)} %broadcast_compare_fusion, f32[4,128]{1,0:T(4,128)S(1)} %convert_bitcast_fusion, bf16[128,4,64]{0,2,1:T(8,128)(2,1)S(1)} %get-tuple-element.246, bf16[4,128,4,64]{1,3,2,0:T(8,128)(2,1)S(1)} %get-tuple-element.244, s32[]{:T(128)} %get-tuple-element.245), kind=kOutput, calls=%fused_computation.14 | convolution fusion | flops 9108992 | bytes 413700 | tf_op jit(solution)/shard_map/while/body/eval_jaxpr/cond/branch_1_fun/qhd,khd->hqk/dot_general | solution.py:15
  46.9 0.7 dynamic_update_slice.22
  48.9 2.6 %conditional.3 = (f32[1,128,256]{1,2,0:T(8,128)S(1)}, f32[1,4,128]{2,1,0:T(4,128)}) conditional(s32[]{:T(128)} %convert_element_type.82, () %tuple.61, (s32[]{:T(128)}, s32[128]{0:T(128)S(1)}, s32[]{:T(128)}, s32[128]{0:T(128)S(1)}, bf16[4,128,4,64]{1,3,2,0:T(8,128)(2,1)S(1)}, /*index=5*/s32[]{:T(128)}, bf16[128,4,64]{0,2,1:T(8,128)(2,1)S(1)}, ...), branch_computations={%region_2.2_spmd, %region_3.4_spmd} | conditional | flops 119505664 | bytes 1179684 | solution.py:76
  49.0 1.0 %fusion.11 = (f32[4,128]{1,0:T(4,128)}, f32[4,128,128]{1,2,0:T(8,128)S(1)}) fusion(pred[128,128]{0,1:T(8,128)(4,1)S(1)} %broadcast_compare_fusion, f32[4,128]{1,0:T(4,128)S(1)} %convert_bitcast_fusion, bf16[128,4,64]{0,2,1:T(8,128)(2,1)S(1)} %get-tuple-element.246, bf16[4,128,4,64]{1,3,2,0:T(8,128)(2,1)S(1)} %get-tuple-element.244, s32[]{:T(128)} %get-tuple-element.245), kind=kOutput, calls=%fused_computation.14 | convolution fusion | flops 9108992 | bytes 413700 | tf_op jit(solution)/shard_map/while/body/eval_jaxpr/cond/branch_1_fun/qhd,khd->hqk/dot_general | solution.py:15
  51.5 0.7 dynamic_update_slice.22
  53.5 2.6 %conditional.3 = (f32[1,128,256]{1,2,0:T(8,128)S(1)}, f32[1,4,128]{2,1,0:T(4,128)}) conditional(s32[]{:T(128)} %convert_element_type.82, () %tuple.61, (s32[]{:T(128)}, s32[128]{0:T(128)S(1)}, s32[]{:T(128)}, s32[128]{0:T(128)S(1)}, bf16[4,128,4,64]{1,3,2,0:T(8,128)(2,1)S(1)}, /*index=5*/s32[]{:T(128)}, bf16[128,4,64]{0,2,1:T(8,128)(2,1)S(1)}, ...), branch_computations={%region_2.2_spmd, %region_3.4_spmd} | conditional | flops 119505664 | bytes 1179684 | solution.py:76
  53.6 1.0 %fusion.11 = (f32[4,128]{1,0:T(4,128)}, f32[4,128,128]{1,2,0:T(8,128)S(1)}) fusion(pred[128,128]{0,1:T(8,128)(4,1)S(1)} %broadcast_compare_fusion, f32[4,128]{1,0:T(4,128)S(1)} %convert_bitcast_fusion, bf16[128,4,64]{0,2,1:T(8,128)(2,1)S(1)} %get-tuple-element.246, bf16[4,128,4,64]{1,3,2,0:T(8,128)(2,1)S(1)} %get-tuple-element.244, s32[]{:T(128)} %get-tuple-element.245), kind=kOutput, calls=%fused_computation.14 | convolution fusion | flops 9108992 | bytes 413700 | tf_op jit(solution)/shard_map/while/body/eval_jaxpr/cond/branch_1_fun/qhd,khd->hqk/dot_general | solution.py:15
  56.1 0.7 dynamic_update_slice.22
  58.1 2.6 %conditional.3 = (f32[1,128,256]{1,2,0:T(8,128)S(1)}, f32[1,4,128]{2,1,0:T(4,128)}) conditional(s32[]{:T(128)} %convert_element_type.82, () %tuple.61, (s32[]{:T(128)}, s32[128]{0:T(128)S(1)}, s32[]{:T(128)}, s32[128]{0:T(128)S(1)}, bf16[4,128,4,64]{1,3,2,0:T(8,128)(2,1)S(1)}, /*index=5*/s32[]{:T(128)}, bf16[128,4,64]{0,2,1:T(8,128)(2,1)S(1)}, ...), branch_computations={%region_2.2_spmd, %region_3.4_spmd} | conditional | flops 119505664 | bytes 1179684 | solution.py:76
  58.2 1.0 %fusion.11 = (f32[4,128]{1,0:T(4,128)}, f32[4,128,128]{1,2,0:T(8,128)S(1)}) fusion(pred[128,128]{0,1:T(8,128)(4,1)S(1)} %broadcast_compare_fusion, f32[4,128]{1,0:T(4,128)S(1)} %convert_bitcast_fusion, bf16[128,4,64]{0,2,1:T(8,128)(2,1)S(1)} %get-tuple-element.246, bf16[4,128,4,64]{1,3,2,0:T(8,128)(2,1)S(1)} %get-tuple-element.244, s32[]{:T(128)} %get-tuple-element.245), kind=kOutput, calls=%fused_computation.14 | convolution fusion | flops 9108992 | bytes 413700 | tf_op jit(solution)/shard_map/while/body/eval_jaxpr/cond/branch_1_fun/qhd,khd->hqk/dot_general | solution.py:15
  60.7 0.7 dynamic_update_slice.22
  61.7 13.7 %all_to_all.16 = bf16[4,32,256]{2,1,0:T(8,128)(2,1)S(1)} all-to-all(bf16[4,32,256]{2,1,0:T(8,128)(2,1)S(1)} %bitcast.54), channel_id=1, replica_groups=mesh['grp'=2,'sp'=4,'tp'=4] {'tp'}, dimensions={0} | all-to-all | bytes 131072 | tf_op jit(solution)/shard_map/all_to_all | solution.py:118
  75.4 3.0 %convolution_convert_fusion = bf16[32,2048]{1,0:T(8,128)(2,1)S(1)} fusion(bf16[32,1024]{1,0:T(8,128)(2,1)S(1)} %bitcast.53, bf16[1024,2048]{1,0:T(8,128)(2,1)} %all-gather.2.cloned.1.call-done), kind=kOutput, calls=%fused_computation.32 | convolution fusion | flops 134283264 | bytes 4390912 | tf_op jit(solution)/shard_map/dot_general | solution.py:120
  78.4 7.3 %all_gather.19 = bf16[128,2048]{1,0:T(8,128)(2,1)S(1)} all-gather(bf16[32,2048]{1,0:T(8,128)(2,1)S(1)} %convolution_convert_fusion), channel_id=1, replica_groups=mesh['grp'=2,'sp'=4,'tp'=4] {'tp'}, dimensions={0}, use_global_device_ids=true | all-gather | bytes 655360 | tf_op jit(solution)/shard_map/all_gather | solution.py:121
  85.7 0.8 copy.73
  (61 shorter events, 10.8 us)
Async XLA Ops:
  6.5 2.0 %copy-start = (bf16[2048,256]{1,0:T(8,128)(2,1)S(1)}, bf16[2048,256]{1,0:T(8,128)(2,1)}, u32[]{:S(2)}) copy-start(bf16[2048,256]{1,0:T(8,128)(2,1)} %param.14) | copy-start | bytes 3145732
  6.5 14.9 %copy-start.1 = (bf16[128,2048]{1,0:T(8,128)(2,1)S(1)}, bf16[128,2048]{1,0:T(8,128)(2,1)}, u32[]{:S(2)}) copy-start(bf16[128,2048]{1,0:T(8,128)(2,1)} %param.11) | copy-start | bytes 1572868
  6.5 14.9 %copy-start.3 = (f32[2048]{0:T(1024)S(1)}, f32[2048]{0:T(1024)}, u32[]{:S(2)}) copy-start(f32[2048]{0:T(1024)} %param.12) | copy-start | bytes 24580
  6.5 68.8 %all-gather.2.cloned.1.call-start = ((), (), s32[]{:S(2)}) async-start(), calls=%async_computation.1 | async-start | bytes 5242880 | tf_op jit(solution)/shard_map/all_gather | solution.py:119
  9.9 27.4 %copy-start.2 = (bf16[4,128]{1,0:T(4,128)(2,1)S(1)}, bf16[4,128]{1,0:T(4,128)(2,1)}, u32[]{:S(2)}) copy-start(bf16[4,128]{1,0:T(4,128)(2,1)} %param.17) | copy-start | bytes 3076
Sparse Core Ops, SparseCore 0:
  8.9 35.8 all-gather.1
where the time goes:
time: 93.8 us; the launch traced here: 93.3 us
  blocking collectives  49.5 us (53%)
  matrix products  14.6 us (16%)
  between operations  13.5 us (14%)
  local copies, waits for them, and re-layouts  7.46 us (8%)
  other arithmetic  4.42 us (5%)
  loops' own time  3.02 us (3%)
    all_to_all x1, blocking collectives, on_device(): lax.all_to_all(mixed, 'tp', split_axis=0, concat_axis=1, tiled=True)  13.7 us
    all_gather x1, blocking collectives, on_device(): piece_values = lax.all_gather(value_rows, 'sp', axis=0, tiled=True)  12 us
    all_gather x1, blocking collectives, on_device(): piece_keys = lax.all_gather(key_rows, 'sp', axis=0, tiled=True)  11 us
    all_gather x1, blocking collectives, on_device(): return lax.all_gather(own_rows, 'tp', axis=0, tiled=True)  7.28 us
    all_gather x1, blocking collectives, on_device(): piece_rates = lax.all_gather(rate_row_values, 'sp', axis=0, tiled=True)  5.6 us
    dot_general x4, matrix products, break_scores(): jnp.einsum('qhd,khd->hqk', query_heads, key_heads, preferred_element_type...  3.93 us
    dot_general x1, matrix products, on_device(): jnp.dot(token_heads, whole_out, preferred_element_type=F32).astype(BF16)  3.01 us
    dynamic_update_slice x4, local copies, waits for them, and re-layouts, absorb_one(): lax.dynamic_update_index_in_dim(inner_pair[1], remain, shard_index, 0)  2.88 us
  transfers between devices with their start and end apart: 1, of which 0 were waited for; matrix products, arithmetic and copies ran while one was open for 24% of the time, Pallas kernels for 0%

commit v1 on v0

--- a/solution.py
+++ b/solution.py
@@ -88,7 +88,24 @@
         jnp.zeros((shard_total, row_count, head_width), F32),
         jnp.zeros((shard_total, heads_local, row_count), F32),
     )
-    piece_keys = lax.all_gather(key_rows, "sp", axis=0, tiled=True)
+
+    def _fit_quotas(x_in):
+        group_axis = "sp"
+        world_n = lax.axis_size(group_axis)
+        fields = list(map(lambda no: (no, (no + 1) % world_n), range(world_n)))
+
+        def strips_all_detail(work_now):
+            if len(work_now) == world_n:
+                return work_now
+            return strips_all_detail([lax.ppermute(work_now[0], group_axis, fields), *work_now])
+
+        return jnp.roll(
+            jnp.concatenate(strips_all_detail([x_in]), 0),
+            (lax.axis_index(group_axis) + 1) * x_in.shape[0],
+            0,
+        )
+
+    piece_keys = _fit_quotas(key_rows)
     piece_values = lax.all_gather(value_rows, "sp", axis=0, tiled=True)
     piece_rates = lax.all_gather(rate_row_values, "sp", axis=0, tiled=True)
     piece_count = piece_keys.shape[0] // row_count

time: 93.8 us -> 88.6 us (0.945)
  blocking collectives: 49.5 us -> 37.5 us
  starting transfers between devices: 0.01 us -> 5.48 us
  waiting for transfers between devices: 0.71 us -> 2.96 us
  matrix products: 14.6 us -> 13.6 us
    all_gather x1 -> x0, blocking collectives: 11 us -> none  [on_device(): piece_keys = lax.all_gather(key_rows, 'sp', axis=0, tiled=True)]
    ppermute x0 -> x3, starting transfers between devices: none -> 5.44 us  [strips_all_detail(): lax.ppermute(work_now[0], group_axis, fields)]
    ppermute x0 -> x3, waiting for transfers between devices: none -> 2.28 us  [strips_all_detail(): lax.ppermute(work_now[0], group_axis, fields)]
    dot_general x1, matrix products: 1.58 us -> 0.36 us  [on_device(): queries = jnp.dot(normed, w_query, preferred_element_type=F32).astype(BF16)]
  transfers between devices with their start and end apart: 1 -> 4, of which waited for: 0 -> 2; matrix products, arithmetic and copies ran while one was open for 24% -> 25% of each run, Pallas kernels for 0% -> 0%
where the time goes in v1:
time: 88.6 us; the launch traced here: 88.2 us
  blocking collectives  37.5 us (42%)
  matrix products  13.6 us (15%)
  between operations  13.6 us (15%)
  local copies, waits for them, and re-layouts  7.5 us (8%)
  starting transfers between devices  5.48 us (6%)
  other arithmetic  4.48 us (5%)
  loops' own time  3.02 us (3%)
  waiting for transfers between devices  2.96 us (3%)
    all_to_all x1, blocking collectives, on_device(): lax.all_to_all(mixed, 'tp', split_axis=0, concat_axis=1, tiled=True)  13.2 us
    all_gather x1, blocking collectives, on_device(): piece_values = lax.all_gather(value_rows, 'sp', axis=0, tiled=True)  11.5 us
    all_gather x1, blocking collectives, on_device(): return lax.all_gather(own_rows, 'tp', axis=0, tiled=True)  7.28 us
    all_gather x1, blocking collectives, on_device(): piece_rates = lax.all_gather(rate_row_values, 'sp', axis=0, tiled=True)  5.6 us
    ppermute x3, starting transfers between devices, strips_all_detail(): lax.ppermute(work_now[0], group_axis, fields)  5.44 us
    dot_general x4, matrix products, break_scores(): jnp.einsum('qhd,khd->hqk', query_heads, key_heads, preferred_element_type...  3.93 us
    dot_general x1, matrix products, on_device(): jnp.dot(token_heads, whole_out, preferred_element_type=F32).astype(BF16)  3.01 us
    dynamic_update_slice x4, local copies, waits for them, and re-layouts, absorb_one(): lax.dynamic_update_index_in_dim(inner_pair[1], remain, shard_index, 0)  2.88 us
  transfers between devices with their start and end apart: 4, of which 2 were waited for; matrix products, arithmetic and copies ran while one was open for 25% of the time, Pallas kernels for 0%

profile of v1, /device:TPU:25, one launch (start us, length us, event | category | flops | bytes accessed | tf_op | source)
XLA Modules:
  0.0 88.2 jit_solution(2794309531280793079)
XLA Ops:
  7.3 1.3 %fusion.25 = f32[128]{0:T(128)S(1)} fusion(bf16[128,2048]{1,0:T(8,128)(2,1)} %param.11), kind=kLoop, calls=%fused_computation.40 | loop fusion | flops 786304 | bytes 524800 | tf_op jit(solution)/shard_map/reduce_sum | solution.py:49
  8.6 1.4 %convolution_convert_fusion.3 = bf16[128,256]{1,0:T(8,128)(2,1)S(1)} fusion(bf16[2048,256]{1,0:T(8,128)(2,1)S(1)} %copy-done, bf16[128,2048]{1,0:T(8,128)(2,1)} %param.11, f32[2048]{0:T(1024)} %param.12, f32[128]{0:T(128)S(1)} %add_rsqrt_fusion), kind=kOutput, calls=%fused_computation.37 | convolution fusion | flops 135299072 | bytes 1647104 | tf_op jit(solution)/shard_map/dot_general | solution.py:53
  10.1 1.8 %convolution_convert_fusion.1 = bf16[128,256]{1,0:T(8,128)(2,1)S(1)} fusion(bf16[2048,256]{1,0:T(8,128)(2,1)} %param.15, bf16[128,2048]{1,0:T(8,128)(2,1)} %param.11, f32[2048]{0:T(1024)} %param.12, f32[128]{0:T(128)S(1)} %add_rsqrt_fusion), kind=kOutput, calls=%fused_computation.35 | convolution fusion | flops 135299072 | bytes 1647104 | tf_op jit(solution)/shard_map/dot_general | solution.py:54
  11.8 1.3 %collective-permute-done = bf16[128,256]{1,0:T(8,128)(2,1)S(1)} collective-permute-done((bf16[128,256]{1,0:T(8,128)(2,1)S(1)}, bf16[128,256]{1,0:T(8,128)(2,1)S(1)}, u32[]{:S(2)}, u32[]{:S(2)}) %collective-permute-start) | collective-permute-done | bytes 65568 | tf_op jit(solution)/shard_map/ppermute | solution.py:100
  13.2 1.8 %collective-permute-start.1 = (bf16[128,256]{1,0:T(8,128)(2,1)S(1)}, bf16[128,256]{1,0:T(8,128)(2,1)S(1)}, u32[]{:S(2)}, u32[]{:S(2)}) collective-permute-start(bf16[128,256]{1,0:T(8,128)(2,1)S(1)} %collective-permute-done), channel_id=1, source_target_pairs={{0,4},{4,8},{8,12},{12,0},{1,5},{5,9},{9,13},{13,1},{2,6},{6,10},{... | collective-permute-start | bytes 196616 | tf_op jit(solution)/shard_map/ppermute | solution.py:100
  15.4 0.9 %collective-permute-done.1 = bf16[128,256]{1,0:T(8,128)(2,1)S(1)} collective-permute-done((bf16[128,256]{1,0:T(8,128)(2,1)S(1)}, bf16[128,256]{1,0:T(8,128)(2,1)S(1)}, u32[]{:S(2)}, u32[]{:S(2)}) %collective-permute-start.1) | collective-permute-done | bytes 65568 | tf_op jit(solution)/shard_map/ppermute | solution.py:100
  16.3 3.6 %collective-permute-start.2 = (bf16[128,256]{1,0:T(8,128)(2,1)S(1)}, bf16[128,256]{1,0:T(8,128)(2,1)S(1)}, u32[]{:S(2)}, u32[]{:S(2)}) collective-permute-start(bf16[128,256]{1,0:T(8,128)(2,1)S(1)} %collective-permute-done.1), channel_id=1, source_target_pairs={{0,4},{4,8},{8,12},{12,0},{1,5},{5,9},{9,13},{13,1},{2,6},{6,10},{... | collective-permute-start | bytes 196616 | tf_op jit(solution)/shard_map/ppermute | solution.py:100
  19.9 11.5 %all_gather.13 = bf16[512,256]{1,0:T(8,128)(2,1)S(1)} all-gather(bf16[128,256]{1,0:T(8,128)(2,1)S(1)} %convolution_convert_fusion.1), channel_id=1, replica_groups=mesh['grp'=2,'sp'=4,'tp'=4] {'sp'}, dimensions={0}, use_global_device_ids=true | all-gather | bytes 327680 | tf_op jit(solution)/shard_map/all_gather | solution.py:109
  32.0 5.6 %all_gather.12 = bf16[512,4]{0,1:T(4,128)(2,1)S(1)} all-gather(bf16[128,4]{0,1:T(4,128)(2,1)S(1)} %bitcast.58), channel_id=1, replica_groups=mesh['grp'=2,'sp'=4,'tp'=4] {'sp'}, dimensions={0}, use_global_device_ids=true | all-gather | bytes 5120 | tf_op jit(solution)/shard_map/all_gather | solution.py:110
  38.4 18.4 %while.16 = (s32[]{:T(128)}, f32[4,128,256]{1,2,0:T(8,128)S(1)}, f32[4,4,128]{2,0,1:T(4,128)S(1)}, s32[4]{0:T(128)S(1)}, s32[]{:T(128)}, /*index=5*/s32[]{:T(128...) while((s32[]{:T(128)}, f32[4,128,256]{1,2,0:T(8,128)S(1)}, ...), condition=%wide.region_5.6_spmd.clone, body=%wide.region_1.5_spmd.clone.sunk | while | flops 119505664 | bytes 1446895 | solution.py:125
  39.6 2.6 %conditional.3 = (f32[1,128,256]{1,2,0:T(8,128)S(1)}, f32[1,4,128]{2,1,0:T(4,128)}) conditional(s32[]{:T(128)} %convert_element_type.82, () %tuple.61, (s32[]{:T(128)}, s32[128]{0:T(128)S(1)}, s32[]{:T(128)}, s32[128]{0:T(128)S(1)}, bf16[4,128,4,64]{1,3,2,0:T(8,128)(2,1)S(1)}, /*index=5*/s32[]{:T(128)}, bf16[128,4,64]{0,2,1:T(8,128)(2,1)S(1)}, ...), branch_computations={%region_2.2_spmd, %region_3.4_spmd} | conditional | flops 119505664 | bytes 1179684 | solution.py:76
  39.8 1.0 %fusion.11 = (f32[4,128]{1,0:T(4,128)}, f32[4,128,128]{1,2,0:T(8,128)S(1)}) fusion(pred[128,128]{0,1:T(8,128)(4,1)S(1)} %broadcast_compare_fusion, f32[4,128]{1,0:T(4,128)S(1)} %convert_bitcast_fusion, bf16[128,4,64]{0,2,1:T(8,128)(2,1)S(1)} %get-tuple-element.246, bf16[4,128,4,64]{1,3,2,0:T(8,128)(2,1)S(1)} %get-tuple-element.244, s32[]{:T(128)} %get-tuple-element.245), kind=kOutput, calls=%fused_computation.14 | convolution fusion | flops 9108992 | bytes 413700 | tf_op jit(solution)/shard_map/while/body/eval_jaxpr/cond/branch_1_fun/qhd,khd->hqk/dot_general | solution.py:15
  42.2 0.7 dynamic_update_slice.22
  44.3 2.6 %conditional.3 = (f32[1,128,256]{1,2,0:T(8,128)S(1)}, f32[1,4,128]{2,1,0:T(4,128)}) conditional(s32[]{:T(128)} %convert_element_type.82, () %tuple.61, (s32[]{:T(128)}, s32[128]{0:T(128)S(1)}, s32[]{:T(128)}, s32[128]{0:T(128)S(1)}, bf16[4,128,4,64]{1,3,2,0:T(8,128)(2,1)S(1)}, /*index=5*/s32[]{:T(128)}, bf16[128,4,64]{0,2,1:T(8,128)(2,1)S(1)}, ...), branch_computations={%region_2.2_spmd, %region_3.4_spmd} | conditional | flops 119505664 | bytes 1179684 | solution.py:76
  44.4 1.0 %fusion.11 = (f32[4,128]{1,0:T(4,128)}, f32[4,128,128]{1,2,0:T(8,128)S(1)}) fusion(pred[128,128]{0,1:T(8,128)(4,1)S(1)} %broadcast_compare_fusion, f32[4,128]{1,0:T(4,128)S(1)} %convert_bitcast_fusion, bf16[128,4,64]{0,2,1:T(8,128)(2,1)S(1)} %get-tuple-element.246, bf16[4,128,4,64]{1,3,2,0:T(8,128)(2,1)S(1)} %get-tuple-element.244, s32[]{:T(128)} %get-tuple-element.245), kind=kOutput, calls=%fused_computation.14 | convolution fusion | flops 9108992 | bytes 413700 | tf_op jit(solution)/shard_map/while/body/eval_jaxpr/cond/branch_1_fun/qhd,khd->hqk/dot_general | solution.py:15
  46.9 0.7 dynamic_update_slice.22
  48.9 2.6 %conditional.3 = (f32[1,128,256]{1,2,0:T(8,128)S(1)}, f32[1,4,128]{2,1,0:T(4,128)}) conditional(s32[]{:T(128)} %convert_element_type.82, () %tuple.61, (s32[]{:T(128)}, s32[128]{0:T(128)S(1)}, s32[]{:T(128)}, s32[128]{0:T(128)S(1)}, bf16[4,128,4,64]{1,3,2,0:T(8,128)(2,1)S(1)}, /*index=5*/s32[]{:T(128)}, bf16[128,4,64]{0,2,1:T(8,128)(2,1)S(1)}, ...), branch_computations={%region_2.2_spmd, %region_3.4_spmd} | conditional | flops 119505664 | bytes 1179684 | solution.py:76
  49.0 1.0 %fusion.11 = (f32[4,128]{1,0:T(4,128)}, f32[4,128,128]{1,2,0:T(8,128)S(1)}) fusion(pred[128,128]{0,1:T(8,128)(4,1)S(1)} %broadcast_compare_fusion, f32[4,128]{1,0:T(4,128)S(1)} %convert_bitcast_fusion, bf16[128,4,64]{0,2,1:T(8,128)(2,1)S(1)} %get-tuple-element.246, bf16[4,128,4,64]{1,3,2,0:T(8,128)(2,1)S(1)} %get-tuple-element.244, s32[]{:T(128)} %get-tuple-element.245), kind=kOutput, calls=%fused_computation.14 | convolution fusion | flops 9108992 | bytes 413700 | tf_op jit(solution)/shard_map/while/body/eval_jaxpr/cond/branch_1_fun/qhd,khd->hqk/dot_general | solution.py:15
  53.5 2.6 %conditional.3 = (f32[1,128,256]{1,2,0:T(8,128)S(1)}, f32[1,4,128]{2,1,0:T(4,128)}) conditional(s32[]{:T(128)} %convert_element_type.82, () %tuple.61, (s32[]{:T(128)}, s32[128]{0:T(128)S(1)}, s32[]{:T(128)}, s32[128]{0:T(128)S(1)}, bf16[4,128,4,64]{1,3,2,0:T(8,128)(2,1)S(1)}, /*index=5*/s32[]{:T(128)}, bf16[128,4,64]{0,2,1:T(8,128)(2,1)S(1)}, ...), branch_computations={%region_2.2_spmd, %region_3.4_spmd} | conditional | flops 119505664 | bytes 1179684 | solution.py:76
  53.6 1.0 %fusion.11 = (f32[4,128]{1,0:T(4,128)}, f32[4,128,128]{1,2,0:T(8,128)S(1)}) fusion(pred[128,128]{0,1:T(8,128)(4,1)S(1)} %broadcast_compare_fusion, f32[4,128]{1,0:T(4,128)S(1)} %convert_bitcast_fusion, bf16[128,4,64]{0,2,1:T(8,128)(2,1)S(1)} %get-tuple-element.246, bf16[4,128,4,64]{1,3,2,0:T(8,128)(2,1)S(1)} %get-tuple-element.244, s32[]{:T(128)} %get-tuple-element.245), kind=kOutput, calls=%fused_computation.14 | convolution fusion | flops 9108992 | bytes 413700 | tf_op jit(solution)/shard_map/while/body/eval_jaxpr/cond/branch_1_fun/qhd,khd->hqk/dot_general | solution.py:15
  57.1 13.2 %all_to_all.16 = bf16[4,32,256]{2,1,0:T(8,128)(2,1)S(1)} all-to-all(bf16[4,32,256]{2,1,0:T(8,128)(2,1)S(1)} %bitcast.54), channel_id=1, replica_groups=mesh['grp'=2,'sp'=4,'tp'=4] {'tp'}, dimensions={0} | all-to-all | bytes 131072 | tf_op jit(solution)/shard_map/all_to_all | solution.py:135
  70.3 3.0 %convolution_convert_fusion = bf16[32,2048]{1,0:T(8,128)(2,1)S(1)} fusion(bf16[32,1024]{1,0:T(8,128)(2,1)S(1)} %bitcast.53, bf16[1024,2048]{1,0:T(8,128)(2,1)} %all-gather.2.cloned.1.call-done), kind=kOutput, calls=%fused_computation.32 | convolution fusion | flops 134283264 | bytes 4390912 | tf_op jit(solution)/shard_map/dot_general | solution.py:137
  73.3 7.3 %all_gather.15 = bf16[128,2048]{1,0:T(8,128)(2,1)S(1)} all-gather(bf16[32,2048]{1,0:T(8,128)(2,1)S(1)} %convolution_convert_fusion), channel_id=1, replica_groups=mesh['grp'=2,'sp'=4,'tp'=4] {'tp'}, dimensions={0}, use_global_device_ids=true | all-gather | bytes 655360 | tf_op jit(solution)/shard_map/all_gather | solution.py:138
  80.5 0.8 copy.79
  (77 shorter events, 12.7 us)
Async XLA Ops:
  6.5 2.1 %copy-start = (bf16[2048,256]{1,0:T(8,128)(2,1)S(1)}, bf16[2048,256]{1,0:T(8,128)(2,1)}, u32[]{:S(2)}) copy-start(bf16[2048,256]{1,0:T(8,128)(2,1)} %param.14) | copy-start | bytes 3145732
  6.5 8.4 %copy-start.1 = (bf16[128,2048]{1,0:T(8,128)(2,1)S(1)}, bf16[128,2048]{1,0:T(8,128)(2,1)}, u32[]{:S(2)}) copy-start(bf16[128,2048]{1,0:T(8,128)(2,1)} %param.11) | copy-start | bytes 1572868
  6.5 8.4 %copy-start.4 = (f32[2048]{0:T(1024)S(1)}, f32[2048]{0:T(1024)}, u32[]{:S(2)}) copy-start(f32[2048]{0:T(1024)} %param.12) | copy-start | bytes 24580
  6.5 8.4 %copy-start.3 = (bf16[2048,256]{1,0:T(8,128)(2,1)S(1)}, bf16[2048,256]{1,0:T(8,128)(2,1)}, u32[]{:S(2)}) copy-start(bf16[2048,256]{1,0:T(8,128)(2,1)} %param.13) | copy-start | bytes 3145732
  6.5 63.7 %all-gather.2.cloned.1.call-start = ((), (), s32[]{:S(2)}) async-start(), calls=%async_computation.1 | async-start | bytes 5242880 | tf_op jit(solution)/shard_map/all_gather | solution.py:136
  7.3 24.7 %copy-start.2 = (bf16[4,128]{1,0:T(4,128)(2,1)S(1)}, bf16[4,128]{1,0:T(4,128)(2,1)}, u32[]{:S(2)}) copy-start(bf16[4,128]{1,0:T(4,128)(2,1)} %param.17) | copy-start | bytes 3076
  10.0 3.2 %collective-permute-start = (bf16[128,256]{1,0:T(8,128)(2,1)S(1)}, bf16[128,256]{1,0:T(8,128)(2,1)S(1)}, u32[]{:S(2)}, u32[]{:S(2)}) collective-permute-start(bf16[128,256]{1,0:T(8,128)(2,1)S(1)} %convolution_convert_fusion.3), channel_id=1, source_target_pairs={{0,4},{4,8},{8,12},{12,0},{1,5},{5,9},{9,13},{13,1},{2,6},{6,10},{... | collective-permute-start | bytes 196616 | tf_op jit(solution)/shard_map/ppermute | solution.py:100
  13.2 3.1 %collective-permute-start.1 = (bf16[128,256]{1,0:T(8,128)(2,1)S(1)}, bf16[128,256]{1,0:T(8,128)(2,1)S(1)}, u32[]{:S(2)}, u32[]{:S(2)}) collective-permute-start(bf16[128,256]{1,0:T(8,128)(2,1)S(1)} %collective-permute-done), channel_id=1, source_target_pairs={{0,4},{4,8},{8,12},{12,0},{1,5},{5,9},{9,13},{13,1},{2,6},{6,10},{... | collective-permute-start | bytes 196616 | tf_op jit(solution)/shard_map/ppermute | solution.py:100
  16.3 21.3 %collective-permute-start.2 = (bf16[128,256]{1,0:T(8,128)(2,1)S(1)}, bf16[128,256]{1,0:T(8,128)(2,1)S(1)}, u32[]{:S(2)}, u32[]{:S(2)}) collective-permute-start(bf16[128,256]{1,0:T(8,128)(2,1)S(1)} %collective-permute-done.1), channel_id=1, source_target_pairs={{0,4},{4,8},{8,12},{12,0},{1,5},{5,9},{9,13},{13,1},{2,6},{6,10},{... | collective-permute-start | bytes 196616 | tf_op jit(solution)/shard_map/ppermute | solution.py:100
Sparse Core Ops, SparseCore 0:
  8.9 35.8 all-gather.1
